TPU v7x, 32 devices: a whole 2x2x4 slice. The times are simulated.
32 devices in a mesh: grp: 2 (over x), fs: 4 (over z), tp: 4 (over y, core).
Axes of the slice: x: 2, y: 2, z: 4, core: 2. Of those that a mesh axis runs over, the one named last changes fastest.
Arguments:
- stream: bfloat16 [2048, 2048], P(('grp', 'fs'), 'tp'), parts along dimension 0, may hold values from -80 to 80
- mixed: bfloat16 [2048, 2048], P(('grp', 'fs'), 'tp'), parts along dimension 0, may hold values from -6 to 6
- out_weight: bfloat16 [2048, 2048], P('fs', 'tp'), may hold values from -0.125 to 0.125
- norm_gain: bfloat16 [2048], P('tp'), may hold values from 0.099609375 to 1.8984375
- up_weight: bfloat16 [2048, 8192], P('fs', 'tp'), may hold values from -0.125 to 0.125
- down_weight: bfloat16 [8192, 2048], P('tp', 'fs'), may hold values from -0.09375 to 0.09375
Outputs:
- result: bfloat16 [2048, 2048], P(('grp', 'fs'), 'tp'), parts along dimension 0
There are 2 independent parts, one for each index of `grp`. A program takes and returns all parts, laid end to end along the dimension named above; an argument that names none is the same for every part. Nothing has to cross between parts.
All inputs are finite; a program needn't handle non-finite values.
Results may differ from a plain program's by a relative error of at most 0.01.
Values may be sent and summed in bfloat16 or wider, within the bound.
A program may use at most 64 MiB of HBM per device.

v0:
```python
import functools

import jax
import jax.numpy as jnp
from jax import lax
from jax.experimental import pallas as pl
from jax.experimental.pallas import tpu as pltpu
from jax.sharding import PartitionSpec as P

epsilon = 1e-06


def fold_product(left, portion):
    return jnp.dot(left, portion, preferred_element_type=jnp.float32)


def gathered_body(stream, mixed, out_weight, norm_gain, up_weight, down_weight):
    mixed_whole = lax.all_gather(mixed, "tp", axis=1, tiled=True)
    projected = fold_product(mixed_whole, lax.all_gather(out_weight, "fs", axis=0, tiled=True))
    resid = (stream.astype(jnp.float32) + projected).astype(jnp.bfloat16)
    widened = resid.astype(jnp.float32)
    resid_whole, gain_whole = (
        lax.all_gather(resid, "tp", axis=1, tiled=True),
        lax.all_gather(norm_gain, "tp", axis=0, tiled=True),
    )
    stream_wide = resid_whole.astype(jnp.float32)
    energy = jnp.mean(stream_wide * stream_wide, axis=1, keepdims=True)
    normed_whole = (
        stream_wide * lax.rsqrt(energy + epsilon) * gain_whole.astype(jnp.float32)
    ).astype(jnp.bfloat16)
    up_full = lax.all_gather(up_weight, "fs", axis=0, tiled=True)
    up_values = jnp.dot(normed_whole, up_full, preferred_element_type=jnp.float32)
    activated = jnp.square(jax.nn.relu(up_values)).astype(jnp.bfloat16)
    partials = jnp.dot(
        activated,
        lax.all_gather(down_weight, "fs", axis=1, tiled=True),
        preferred_element_type=jnp.float32,
    )
    branch = lax.psum_scatter(partials, "tp", scatter_dimension=1, tiled=True)
    return (widened + branch).astype(jnp.bfloat16)


def spread_body(stream, mixed, out_weight, norm_gain, up_weight, down_weight):
    mixed_whole = lax.all_gather(mixed, "tp", axis=1, tiled=True)
    out_full = lax.all_gather(out_weight, "fs", axis=0, tiled=True)
    up_mine = lax.all_to_all(up_weight, "fs", split_axis=1, concat_axis=0, tiled=True)
    down_mine = lax.all_to_all(down_weight, "fs", split_axis=0, concat_axis=1, tiled=True)
    projected = jnp.dot(mixed_whole, out_full, preferred_element_type=jnp.float32)
    resid = (stream.astype(jnp.float32) + projected).astype(jnp.bfloat16)
    rows = lax.all_gather(resid, "fs", axis=0, tiled=True)
    whole = lax.all_gather(rows, "tp", axis=1, tiled=True).astype(jnp.float32)
    gain = lax.all_gather(norm_gain, "tp", axis=0, tiled=True).astype(jnp.float32)
    energy = jnp.mean(whole * whole, axis=1, keepdims=True)
    normed = (whole * lax.rsqrt(energy + epsilon) * gain).astype(jnp.bfloat16)
    up_values = jnp.dot(normed, up_mine, preferred_element_type=jnp.float32)
    activated = jnp.square(jax.nn.relu(up_values)).astype(jnp.bfloat16)
    partials = jnp.dot(activated, down_mine, preferred_element_type=jnp.float32).astype(jnp.bfloat16)
    columns = lax.psum_scatter(partials, "tp", scatter_dimension=1, tiled=True)
    branch = lax.psum_scatter(columns, "fs", scatter_dimension=0, tiled=True)
    return (resid.astype(jnp.float32) + branch.astype(jnp.float32)).astype(jnp.bfloat16)


MESH = pl.DeviceIdType.MESH


def slot_table(fs):
    table, count = {}, 0
    hops = 2 * (fs - 1)
    sizes = dict(
        mixed=3, gain=3, out_z=hops, out_x=hops, up_z=fs, up_x=fs, down_z=fs, down_x=fs,
        rows_z=hops, rows_y=hops + 1, rows_c=hops + 1, rows_d=hops + 1,
        sum_c=fs * fs, sum_y=fs, sum_z=fs,
    )
    for name, size in sizes.items():
        table[name] = count
        count += size
    return table, count


def layer_kernel(
    fs, slots,
    stream_ref, mixed_ref, out_ref, gain_ref, up_ref, down_ref, result_ref,
    mixw, gains, wo, wup, wdn, rows, acts, kept, mine, send_c, got_c, send_y, got_y, send_z, got_z,
    send_sem, recv_sem, local_sem,
):
    f32, bf16 = jnp.float32, jnp.bfloat16
    g, i, j = lax.axis_index("grp"), lax.axis_index("fs"), lax.axis_index("tp")
    y, c = j // 2, j % 2
    jc = y * 2 + (1 - c)
    jy = (1 - y) * 2 + c
    jd = (1 - y) * 2 + (1 - c)
    half, width = wo.shape[2], wo.shape[3]
    order = [s for s in (2, 1, 3) if s < fs] if fs == 4 else list(range(1, fs))

    core, across, diag, twin = (g, i, jc), (g, i, jy), (g, i, jd), (1 - g, i, j)

    def ahead(s):
        return lax.rem(i + s, fs)

    def behind(s):
        return lax.rem(i + fs - s, fs)

    def slice_of(s):
        return (g, ahead(s), j)

    sent = []

    def copy(name, k, src, dst, target):
        n = slots[name] + k
        return pltpu.make_async_remote_copy(
            src_ref=src, dst_ref=dst, send_sem=send_sem.at[n], recv_sem=recv_sem.at[n],
            device_id=target, device_id_type=MESH,
        )

    def send(name, k, src, dst, target, given=None):
        made = copy(name, k, src, dst, target)
        made.start()
        sent.append((made, None) if given is None else ((name, k), given))

    both = jnp.logical_and

    hops = [(side, d) for d in range(1, fs) for side in range(2)]

    def hop(side, d):
        return side * (fs - 1) + d - 1

    def neighbour(side):
        return slice_of(1) if side == 0 else slice_of(fs - 1)

    def onward(side):
        return i < fs - 1 if side == 0 else i > 0

    def start_relay(name, src, dst):
        for side in range(2):
            @pl.when(onward(side))
            def _():
                send(name, hop(side, 1), src, dst, neighbour(side), lambda side=side: onward(side))

    def take_relay(name, side, d, block_of, then):
        has = i >= d if side == 0 else i + d < fs
        b = i - d if side == 0 else i + d

        @pl.when(has)
        def _():
            arrive(name, hop(side, d), block_of(b), neighbour(1 - side))
            if d < fs - 1:
                @pl.when(onward(side))
                def _():
                    send(
                        name, hop(side, d + 1), block_of(b), block_of(b), neighbour(side),
                        lambda: both(has, onward(side)),
                    )
            then(b, hop(side, d), lambda: has)

    def arrive(name, k, dst, target):
        copy(name, k, dst, dst, target).wait_recv()

    barrier = pltpu.get_barrier_semaphore()
    greeted = [core, across, diag, twin] + [slice_of(s) for s in order]
    for device in greeted:
        pl.semaphore_signal(barrier, inc=1, device_id=device, device_id_type=MESH)

    local = []

    def keep(src, dst):
        made = pltpu.make_async_copy(src, dst, local_sem.at[len(local)])
        made.start()
        local.append(made)

    def up_piece(owner, part):
        return up_ref.at[pl.ds(part * half, half), pl.ds(pl.multiple_of(owner * width, width), width)]

    def down_piece(owner, part):
        return down_ref.at[pl.ds(owner * 2 * half + part * half, half), :]

    for part in range(2):
        keep(out_ref.at[pl.ds(part * half, half), :], wo.at[i, part])
        keep(up_piece(i, part), wup.at[i, part])
        keep(down_piece(i, part), wdn.at[i, part])
    keep(mixed_ref, mixw.at[j])
    keep(gain_ref, gains.at[j])
    pl.semaphore_wait(barrier, len(greeted))

    send("mixed", 0, mixed_ref, mixw.at[j], across)
    send("mixed", 1, mixed_ref, mixw.at[j], core)
    start_relay("out_z", out_ref.at[pl.ds(g * half, half), :], wo.at[i, g])
    send("gain", 0, gain_ref, gains.at[j], across)
    send("gain", 1, gain_ref, gains.at[j], core)
    send("gain", 2, gain_ref, gains.at[j], diag)

    def out_block(b):
        return wo.at[b, g]

    def out_cross(b, n, has):
        send("out_x", n, out_block(b), out_block(b), twin, has)

    for side, d in hops:
        if d == fs - 1 and side == 0:
            for s in order:
                send("up_z", s, up_piece(ahead(s), g), wup.at[i, g], slice_of(s))
        take_relay("out_z", side, d, out_block, out_cross)
    arrive("mixed", 0, mixw.at[jy], across)
    send("mixed", 2, mixw.at[jy], mixw.at[jy], core)
    arrive("mixed", 1, mixw.at[jc], core)
    arrive("mixed", 2, mixw.at[jd], core)
    for made in local:
        made.wait()

    def whole(ref, k):
        return ref[k].reshape(2 * half, width)

    for side, d in hops:
        has = i >= d if side == 0 else i + d < fs
        b = i - d if side == 0 else i + d

        @pl.when(has)
        def _():
            arrive("out_x", hop(side, d), wo.at[b, 1 - g], twin)

    total = stream_ref[...].astype(f32)
    for k in range(fs):
        total += jnp.dot(mixw[k], whole(wo, k), preferred_element_type=f32)
    rows[j, i] = total.astype(bf16)

    start_relay("rows_z", rows.at[j, i], rows.at[j, i])
    send("rows_y", 0, rows.at[j, i], rows.at[j, i], across)
    send("rows_c", 0, rows.at[j, i], rows.at[j, i], core)

    for s in order:
        b = behind(s)
        arrive("up_z", s, wup.at[b, g], slice_of(s))
        send("up_x", s, wup.at[b, g], wup.at[b, g], twin)
    arrive("rows_y", 0, rows.at[jy, i], across)
    send("rows_d", 0, rows.at[jy, i], rows.at[jy, i], core)

    def rows_block(b):
        return rows.at[j, b]

    def rows_cross(b, n, has):
        send("rows_y", n + 1, rows_block(b), rows_block(b), across, has)
        send("rows_c", n + 1, rows_block(b), rows_block(b), core, has)

    for side, d in hops:
        if d == fs - 1 and side == 0:
            for s in order:
                send("down_z", s, down_piece(ahead(s), g), wdn.at[i, g], slice_of(s))
        take_relay("rows_z", side, d, rows_block, rows_cross)
    arrive("gain", 0, gains.at[jy], across)
    arrive("gain", 1, gains.at[jc], core)
    arrive("gain", 2, gains.at[jd], diag)
    for s in order:
        arrive("up_x", s, wup.at[behind(s), 1 - g], twin)

    def hidden(t):
        wide = [rows[k, t].astype(f32) for k in range(rows.shape[0])]
        energy = sum(jnp.sum(w * w, axis=1, keepdims=True) for w in wide)
        scale = lax.rsqrt(energy * (1.0 / (len(wide) * width)) + epsilon)
        up = None
        for k, w in enumerate(wide):
            normed = (w * scale * gains[k].astype(f32)).astype(bf16)
            term = jnp.dot(normed, whole(wup, k), preferred_element_type=f32)
            up = term if up is None else up + term
        return jnp.square(jnp.maximum(up, 0.0)).astype(bf16)

    def cross_down(s):
        arrive("down_z", s, wdn.at[behind(s), g], slice_of(s))
        send("down_x", s, wdn.at[behind(s), g], wdn.at[behind(s), g], twin)

    arrive("rows_c", 0, rows.at[jc, i], core)
    arrive("rows_d", 0, rows.at[jd, i], core)
    acts[i] = hidden(i)
    for side, d in hops:
        has = i >= d if side == 0 else i + d < fs
        b = i - d if side == 0 else i + d
        n = hop(side, d) + 1
        if d == fs - 1 and side == 0:
            cross_down(order[0])

        @pl.when(has)
        def _():
            arrive("rows_y", n, rows.at[jy, b], across)
            send("rows_d", n, rows.at[jy, b], rows.at[jy, b], core, lambda has=has: has)
            arrive("rows_c", n, rows.at[jc, b], core)
            arrive("rows_d", n, rows.at[jd, b], core)
            acts[b] = hidden(b)

    last = order + [0]

    def column(n, k):
        ck, yk = k % 2, k // 2
        w = whole(wdn, k)

        @pl.when(ck != c)
        def _():
            for s in last:
                t = ahead(s)
                send_c[yk, t] = jnp.dot(acts[t], w, preferred_element_type=f32).astype(bf16)
                send("sum_c", n * fs + s, send_c.at[yk, t], got_c.at[yk, t], core, lambda: ck != c)

        @pl.when(ck == c)
        def _():
            for s in last:
                t = ahead(s)
                part = jnp.dot(acts[t], w, preferred_element_type=f32)
                arrive("sum_c", n * fs + s, got_c.at[yk, t], core)
                kept[t] = part + got_c[yk, t].astype(f32)

                @pl.when(yk != y)
                def _():
                    send_y[t] = kept[t].astype(bf16)
                    send("sum_y", s, send_y.at[t], got_y.at[t], across, lambda: both(ck == c, yk != y))

                @pl.when(yk == y)
                def _():
                    mine[t] = kept[t]

    def owned(given):
        @pl.when(given)
        def _():
            for s in order:
                t = ahead(s)
                arrive("sum_y", s, got_y.at[t], across)
                send_z[t] = (mine[t] + got_y[t].astype(f32)).astype(bf16)
                send("sum_z", s, send_z.at[t], got_z.at[i], slice_of(s), lambda: given)

    early = jnp.logical_or(behind(0) == j, behind(order[0]) == j)
    for n, s in enumerate([0] + order):
        if 0 < n < len(order):
            cross_down(order[n])
        if s > 0:
            arrive("down_x", s, wdn.at[behind(s), 1 - g], twin)
        column(n, behind(s))
        if n == len(order) - 1:
            owned(early)
    owned(jnp.logical_not(early))
    arrive("sum_y", 0, got_y.at[i], across)
    branch = mine[i] + got_y[i].astype(f32)
    for s in order:
        b = behind(s)
        arrive("sum_z", s, got_z.at[b], slice_of(s))
        branch += got_z[b].astype(f32)
    result_ref[...] = (rows[j, i].astype(f32) + branch).astype(bf16)
    for made, given in sent:
        if given is None:
            made.wait_send()
        else:
            block = wo.at[0, 0] if made[0].startswith("out") else rows.at[0, 0]
            pl.when(given())(copy(*made, block, block, core).wait_send)


def kernel_body(fs, tp, stream, mixed, out_weight, norm_gain, up_weight, down_weight):
    tokens, width = stream.shape
    half = out_weight.shape[0] // 2
    slots, count = slot_table(fs)
    vmem, anywhere = pl.BlockSpec(memory_space=pltpu.VMEM), pl.BlockSpec(memory_space=pl.ANY)
    weights = pltpu.VMEM((fs, 2, half, width), jnp.bfloat16)
    blocks = pltpu.VMEM((fs, tokens, width), jnp.bfloat16)
    columns = pltpu.VMEM((2, fs, tokens, width), jnp.bfloat16)
    sums = pltpu.VMEM((fs, tokens, width), jnp.float32)
    return pl.pallas_call(
        functools.partial(layer_kernel, fs, slots),
        out_shape=jax.ShapeDtypeStruct((tokens, width), jnp.bfloat16),
        in_specs=[vmem, vmem, anywhere, vmem, anywhere, anywhere],
        out_specs=vmem,
        scratch_shapes=[
            pltpu.VMEM((tp, tokens, width), jnp.bfloat16),
            pltpu.VMEM((tp, 1, width), jnp.bfloat16),
            weights, weights, weights,
            pltpu.VMEM((tp, fs, tokens, width), jnp.bfloat16),
            blocks,
            sums, sums,
            columns, columns, blocks, blocks, blocks, blocks,
            pltpu.SemaphoreType.DMA((count,)),
            pltpu.SemaphoreType.DMA((count,)),
            pltpu.SemaphoreType.DMA((8,)),
        ],
        compiler_params=pltpu.CompilerParams(
            collective_id=0, has_side_effects=True, vmem_limit_bytes=56 * 1024 * 1024
        ),
    )(stream, mixed, out_weight, norm_gain.reshape(1, width), up_weight, down_weight)


def solution(mesh):
    placed = (
        P(("grp", "fs"), "tp"),
        P(("grp", "fs"), "tp"),
        P("fs", "tp"),
        P("tp"),
        P("fs", "tp"),
        P("tp", "fs"),
    )
    fs, tp = mesh.shape["fs"], mesh.shape["tp"]

    def call(stream, mixed, out_weight, norm_gain, up_weight, down_weight):
        width, hidden = up_weight.shape
        tokens = stream.shape[0] // mesh.shape["grp"]
        moved_weights = 2 * width * hidden // tp
        moved_rows = 2 * tokens * width + 2 * width * hidden // (tp * fs)
        aligned = fs == tp == 4 and (width // tp) % 256 == 0 and (tokens // fs) % 16 == 0
        aligned = aligned and hidden == tp * width
        body = spread_body if moved_rows < moved_weights else gathered_body
        if aligned and moved_rows < moved_weights:
            body = functools.partial(kernel_body, fs, tp)
        return sharded(body)(stream, mixed, out_weight, norm_gain, up_weight, down_weight)

    def sharded(body):
        return jax.shard_map(
            body, mesh=mesh, in_specs=placed, out_specs=P(("grp", "fs"), "tp"), check_vma=False
        )

    return call
```

profile of v0, /device:TPU:1, one launch (start us, length us, event | category | flops | bytes accessed | tf_op | source)
XLA Modules:
  0.0 124.3 jit_solution(1406589503927454738)
XLA Ops:
  0.0 1.3 %reshape.3.gain_ref = bf16[1,512]{1,0:T(2,128)(2,1)} reshape(bf16[512]{0:T(512)(128)(2,1)} %param.9) | data formatting | bytes 2048 | tf_op jit(solution)/shard_map/reshape | solution.py:380
  1.3 121.4 %shard_map.64 = bf16[256,512]{1,0:T(8,128)(2,1)} custom-call(bf16[256,512]{1,0:T(8,128)(2,1)} %stream_ref.1, bf16[256,512]{1,0:T(8,128)(2,1)} %mixed_ref.1, bf16[512,512]{1,0:T(8,128)(2,1)} %out_ref.1, bf16[1,512]{1,0:T(2,128)(2,1)} %reshape.3.gain_ref, bf16[512,2048]{1,0:T(8,128)(2,1)} %up_ref.1, bf16[2048,512]{1,0:T(8,128)(2,1)} %down_ref.1), custom_call_target="tpu_custom_call" | custom-call | tf_op jit(solution)/shard_map/pallas_call | solution.py:360
  122.6 1.7 %copy.8 = bf16[256,512]{1,0:T(8,128)(2,1)} copy(bf16[256,512]{1,0:T(8,128)(2,1)} %shard_map.64) | data formatting | bytes 524288
where the time goes:
time: 124 us
  Pallas kernels  121 us (98%)
  local copies, waits for them, and re-layouts  2.93 us (2%)
    pallas_call x1, Pallas kernels, kernel_body(): pl.pallas_call(functools.partial(layer_kernel, fs, slots), out_shape=jax....  121 us

commit v1 on v0

v1 whole, which is shorter than its diff:
```python
import functools

import jax
import jax.numpy as jnp
from jax import lax
from jax.experimental import pallas as pl
from jax.experimental.pallas import tpu as pltpu
from jax.sharding import PartitionSpec as P

epsilon = 1e-06


def fold_product(left, portion):
    return jnp.dot(left, portion, preferred_element_type=jnp.float32)


def gathered_body(stream, mixed, out_weight, norm_gain, up_weight, down_weight):
    mixed_whole = lax.all_gather(mixed, "tp", axis=1, tiled=True)
    projected = fold_product(mixed_whole, lax.all_gather(out_weight, "fs", axis=0, tiled=True))
    resid = (stream.astype(jnp.float32) + projected).astype(jnp.bfloat16)
    widened = resid.astype(jnp.float32)
    resid_whole, gain_whole = (
        lax.all_gather(resid, "tp", axis=1, tiled=True),
        lax.all_gather(norm_gain, "tp", axis=0, tiled=True),
    )
    stream_wide = resid_whole.astype(jnp.float32)
    energy = jnp.mean(stream_wide * stream_wide, axis=1, keepdims=True)
    normed_whole = (
        stream_wide * lax.rsqrt(energy + epsilon) * gain_whole.astype(jnp.float32)
    ).astype(jnp.bfloat16)
    up_full = lax.all_gather(up_weight, "fs", axis=0, tiled=True)
    up_values = jnp.dot(normed_whole, up_full, preferred_element_type=jnp.float32)
    activated = jnp.square(jax.nn.relu(up_values)).astype(jnp.bfloat16)
    partials = jnp.dot(
        activated,
        lax.all_gather(down_weight, "fs", axis=1, tiled=True),
        preferred_element_type=jnp.float32,
    )
    branch = lax.psum_scatter(partials, "tp", scatter_dimension=1, tiled=True)
    return (widened + branch).astype(jnp.bfloat16)


def spread_body(stream, mixed, out_weight, norm_gain, up_weight, down_weight):
    mixed_whole = lax.all_gather(mixed, "tp", axis=1, tiled=True)
    out_full = lax.all_gather(out_weight, "fs", axis=0, tiled=True)
    up_mine = lax.all_to_all(up_weight, "fs", split_axis=1, concat_axis=0, tiled=True)
    down_mine = lax.all_to_all(down_weight, "fs", split_axis=0, concat_axis=1, tiled=True)
    projected = jnp.dot(mixed_whole, out_full, preferred_element_type=jnp.float32)
    resid = (stream.astype(jnp.float32) + projected).astype(jnp.bfloat16)
    rows = lax.all_gather(resid, "fs", axis=0, tiled=True)
    whole = lax.all_gather(rows, "tp", axis=1, tiled=True).astype(jnp.float32)
    gain = lax.all_gather(norm_gain, "tp", axis=0, tiled=True).astype(jnp.float32)
    energy = jnp.mean(whole * whole, axis=1, keepdims=True)
    normed = (whole * lax.rsqrt(energy + epsilon) * gain).astype(jnp.bfloat16)
    up_values = jnp.dot(normed, up_mine, preferred_element_type=jnp.float32)
    activated = jnp.square(jax.nn.relu(up_values)).astype(jnp.bfloat16)
    partials = jnp.dot(activated, down_mine, preferred_element_type=jnp.float32).astype(jnp.bfloat16)
    columns = lax.psum_scatter(partials, "tp", scatter_dimension=1, tiled=True)
    branch = lax.psum_scatter(columns, "fs", scatter_dimension=0, tiled=True)
    return (resid.astype(jnp.float32) + branch.astype(jnp.float32)).astype(jnp.bfloat16)


MESH = pl.DeviceIdType.MESH


PARTS = dict(out=2, up=2, down=2, rows=2)


def slot_table(fs):
    table, count = {}, 0
    sizes = dict(mixed=3, gain=3, sum_c=fs * fs, sum_y=fs, sum_z=fs)
    for name, parts in PARTS.items():
        sizes[name + "_z"] = 2 * fs * parts
        for way in ("_x",) if name != "rows" else ("_y", "_c", "_d"):
            sizes[name + way] = fs * parts
    for name, size in sizes.items():
        table[name] = count
        count += size
    return table, count


def layer_kernel(
    fs, slots,
    stream_ref, mixed_ref, out_ref, gain_ref, up_ref, down_ref, result_ref,
    mixw, gains, wo, wup, wdn, rows, acts, kept, mine, send_c, got_c, send_y, got_y, send_z, got_z,
    held, send_sem, recv_sem, local_sem,
):
    f32, bf16 = jnp.float32, jnp.bfloat16
    g, i, j = lax.axis_index("grp"), lax.axis_index("fs"), lax.axis_index("tp")
    y, c = j // 2, j % 2
    jc = y * 2 + (1 - c)
    jy = (1 - y) * 2 + c
    jd = (1 - y) * 2 + (1 - c)
    half, width = wo.shape[2], wo.shape[3]

    core, across, diag, twin = (g, i, jc), (g, i, jy), (g, i, jd), (1 - g, i, j)
    both = jnp.logical_and

    def at(z):
        return (g, z, j)

    sent = []

    def copy(name, src, dst, target, sk, rk):
        return pltpu.make_async_remote_copy(
            src_ref=src, dst_ref=dst,
            send_sem=send_sem.at[slots[name] + sk], recv_sem=recv_sem.at[slots[name] + rk],
            device_id=target, device_id_type=MESH,
        )

    def send(name, src, dst, target, sk, rk, given=None):
        def go():
            copy(name, src, dst, target, sk, rk).start()

        if given is None:
            go()
        else:
            pl.when(given)(go)
        sent.append((name, sk, dst, given))

    def arrive(name, rk, dst):
        copy(name, dst, dst, core, rk, rk).wait_recv()

    def has(side, d):
        return i >= d if side == 0 else i + d < fs

    def source(side, d):
        return i - d if side == 0 else i + d

    def goes(side, d):
        return has(1 - side, d)

    def dest(side, d):
        return source(1 - side, d)

    def piece(ref, q, parts):
        size = ref.shape[0] // parts
        return ref.at[pl.ds(q * size, size), :]

    def relay_send(name, block_of, b, side, q, given):
        parts = PARTS[name]
        block = piece(block_of(b), q, parts)
        send(name + "_z", block, block, at(dest(side, 1)), (side * fs + b) * parts + q, b * parts + q, given)

    def relay(name, block_of, d, then):
        parts = PARTS[name]
        for q in range(parts):
            for side in range(2):
                b = source(side, d)
                given = has(side, d)

                @pl.when(given)
                def _():
                    arrive(name + "_z", b * parts + q, piece(block_of(b), q, parts))

                if d < fs - 1:
                    relay_send(name, block_of, b, side, q, both(given, goes(side, 1)))
                then(b, q, given)

    greeted = [core, across, diag, twin]
    barrier = pltpu.get_barrier_semaphore()
    for device in greeted:
        pl.semaphore_signal(barrier, inc=1, device_id=device, device_id_type=MESH)
    for s in range(1, fs):
        pl.semaphore_signal(barrier, inc=1, device_id=at(lax.rem(i + s, fs)), device_id_type=MESH)

    local = []

    def keep(src, dst):
        made = pltpu.make_async_copy(src, dst, local_sem.at[len(local)])
        made.start()
        local.append(made)

    def up_piece(owner, part):
        return up_ref.at[pl.ds(part * half, half), pl.ds(pl.multiple_of(owner * width, width), width)]

    def down_piece(owner, part):
        return down_ref.at[pl.ds(owner * 2 * half + part * half, half), :]

    for part in range(2):
        keep(out_ref.at[pl.ds(part * half, half), :], wo.at[i, part])
        keep(up_piece(i, part), wup.at[i, part])
        keep(down_piece(i, part), wdn.at[i, part])
    keep(mixed_ref, mixw.at[j])
    keep(stream_ref, held)
    gains[j] = gain_ref[...].astype(f32).reshape(1, width).astype(bf16)
    pl.semaphore_wait(barrier, len(greeted) + fs - 1)

    def exchange(name, piece_of, buffer, side, d, given):
        parts = PARTS[name]
        to = dest(side, d)
        for q in range(parts):
            send(
                name + "_z", piece(piece_of(to, g), q, parts), piece(buffer.at[i, g], q, parts), at(to),
                (side * fs + d) * parts + q, i * parts + q, both(given, goes(side, d)),
            )

    def take(name, buffer, b, given=None):
        parts = PARTS[name]
        for q in range(parts):
            block = piece(buffer.at[b, g], q, parts)

            def go():
                arrive(name + "_z", b * parts + q, block)

            if given is None:
                go()
            else:
                pl.when(given)(go)
            send(name + "_x", block, block, twin, b * parts + q, b * parts + q, given)

    def take_x(name, buffer, b):
        parts = PARTS[name]
        for q in range(parts):
            arrive(name + "_x", b * parts + q, piece(buffer.at[b, 1 - g], q, parts))

    def out_block(b):
        return wo.at[b, g]

    parts = PARTS["out"]
    own = out_ref.at[pl.ds(g * half, half), :]
    for q in range(parts):
        for side in range(2):
            send(
                "out_z", piece(own, q, parts), piece(wo.at[i, g], q, parts), at(dest(side, 1)),
                (side * fs + i) * parts + q, i * parts + q, goes(side, 1),
            )
    send("mixed", mixed_ref, mixw.at[j], across, 0, 0)
    send("mixed", mixed_ref, mixw.at[j], core, 1, 1)
    send("gain", gains.at[j], gains.at[j], across, 0, 0)
    send("gain", gains.at[j], gains.at[j], core, 1, 1)
    send("gain", gains.at[j], gains.at[j], diag, 2, 2)

    def ends(side, p):
        return i == p if side == 0 else i == fs - 1 - p

    def out_cross(b, q, given):
        block = piece(wo.at[b, g], q, PARTS["out"])
        n = b * PARTS["out"] + q
        send("out_x", block, block, twin, n, n, given)

    for d in range(fs):
        if d > 0:
            relay("out", out_block, d, out_cross)
        if d == 1:
            arrive("mixed", 0, mixw.at[jy])
            send("mixed", mixw.at[jy], mixw.at[jy], core, 2, 2)
        for side in range(2):
            for e in range(1, fs - d):
                exchange("up", up_piece, wup, side, e, ends(side, d))
    arrive("mixed", 1, mixw.at[jc])
    arrive("mixed", 2, mixw.at[jd])
    for made in local:
        made.wait()

    def whole(ref, k):
        return ref[k].reshape(2 * half, width)

    near = [(side, d) for d in range(1, fs) for side in range(2)]
    for side, d in near:
        @pl.when(has(side, d))
        def _():
            take_x("out", wo, source(side, d))

    total = held[...].astype(f32)
    for k in range(fs):
        total += jnp.dot(mixw[k], whole(wo, k), preferred_element_type=f32)
    rows[j, i] = total.astype(bf16)

    def rows_block(b):
        return rows.at[j, b]

    def rows_cross(b, q, given):
        parts = PARTS["rows"]
        block = piece(rows.at[j, b], q, parts)
        n = b * parts + q
        send("rows_y", block, block, across, n, n, given)
        send("rows_c", block, block, core, n, n, given)

    def rows_fetch(b):
        parts = PARTS["rows"]
        for q in range(parts):
            block = piece(rows.at[jy, b], q, parts)
            n = b * parts + q
            arrive("rows_y", n, block)
            copy("rows_d", block, block, core, n, n).start()

    def rows_sent(b, given):
        parts = PARTS["rows"]
        for q in range(parts):
            sent.append(("rows_d", b * parts + q, piece(rows.at[jy, b], q, parts), given))

    def rows_ready(b):
        parts = PARTS["rows"]
        for q in range(parts):
            n = b * parts + q
            arrive("rows_c", n, piece(rows.at[jc, b], q, parts))
            arrive("rows_d", n, piece(rows.at[jd, b], q, parts))

    for q in range(PARTS["rows"]):
        for side in range(2):
            relay_send("rows", rows_block, i, side, q, goes(side, 1))
        rows_cross(i, q, None)

    def down_issue(d):
        for side in range(2):
            for e in range(1, fs):
                for p in range(fs - e):
                    if max(p, 0 if e == 1 else e) == d:
                        exchange("down", down_piece, wdn, side, e, ends(side, p))

    down_issue(0)

    def hidden(t):
        wide = [rows[k, t].astype(f32) for k in range(rows.shape[0])]
        energy = sum(jnp.sum(w * w, axis=1, keepdims=True) for w in wide)
        scale = lax.rsqrt(energy * (1.0 / (len(wide) * width)) + epsilon)
        up = None
        for k, w in enumerate(wide):
            normed = (w * scale * gains[k].astype(f32)).astype(bf16)
            term = jnp.dot(normed, whole(wup, k), preferred_element_type=f32)
            up = term if up is None else up + term
        acts[t] = jnp.square(jnp.maximum(up, 0.0)).astype(bf16)

    for side, d in near:
        if d == 2 and side == 0:
            rows_fetch(i)
            rows_sent(i, None)
        take("up", wup, source(side, d), has(side, d))

    relay("rows", rows_block, 1, rows_cross)
    down_issue(1)
    arrive("gain", 0, gains.at[jy])
    arrive("gain", 1, gains.at[jc])
    arrive("gain", 2, gains.at[jd])
    for side, d in near:
        @pl.when(has(side, d))
        def _():
            take_x("up", wup, source(side, d))

    def fetch(side, d):
        given = has(side, d)
        pl.when(given)(lambda: rows_fetch(source(side, d)))
        rows_sent(source(side, d), given)

    def digest(side, d):
        @pl.when(has(side, d))
        def _():
            rows_ready(source(side, d))
            hidden(source(side, d))

    rows_ready(i)
    hidden(i)
    relay("rows", rows_block, 2, rows_cross)
    down_issue(2)
    fetch(0, 1)
    fetch(1, 1)
    digest(0, 1)
    relay("rows", rows_block, 3, rows_cross)
    down_issue(3)
    fetch(0, 2)
    fetch(1, 2)
    digest(1, 1)

    low = i < fs // 2
    m = jnp.where(low, i, fs - 1 - i)

    def column_of(n):
        f = jnp.where(m == 0, n, [1, 0, 2, 3][n])
        return jnp.where(low, f, fs - 1 - f)

    def token_of(n):
        f = jnp.where(m == 0, fs - 1 - n, [3, 2, 0, 1][n])
        return jnp.where(low, f, fs - 1 - f)

    fetch(0, 3)
    fetch(1, 3)
    digest(0, 2)
    digest(1, 2)
    digest(0, 3)
    digest(1, 3)

    def column(n):
        k = column_of(n)
        ck, yk = k % 2, k // 2
        w = whole(wdn, k)

        @pl.when(ck != c)
        def _():
            for s in range(fs):
                t = token_of(s)
                send_c[yk, t] = jnp.dot(acts[t], w, preferred_element_type=f32).astype(bf16)
                copy("sum_c", send_c.at[yk, t], got_c.at[yk, t], core, n * fs + s, n * fs + s).start()

        for s in range(fs):
            sent.append(("sum_c", n * fs + s, send_c.at[0, 0], ck != c))

        @pl.when(ck == c)
        def _():
            for s in range(fs):
                t = token_of(s)
                part = jnp.dot(acts[t], w, preferred_element_type=f32)
                arrive("sum_c", n * fs + s, got_c.at[yk, t])
                kept[t] = part + got_c[yk, t].astype(f32)

                @pl.when(yk != y)
                def _():
                    send_y[t] = kept[t].astype(bf16)
                    copy("sum_y", send_y.at[t], got_y.at[t], across, s, s).start()

                @pl.when(yk == y)
                def _():
                    mine[t] = kept[t]

        for s in range(fs):
            if n == 0:
                sent.append(("sum_y", s, send_y.at[0], None))

    def owned(n):
        @pl.when(column_of(n) == j)
        def _():
            for s in range(fs - 1):
                t = token_of(s)
                arrive("sum_y", s, got_y.at[t])
                send_z[t] = (mine[t] + got_y[t].astype(f32)).astype(bf16)
                copy("sum_z", send_z.at[t], got_z.at[i], at(t), t, i).start()

    take("down", wdn, column_of(1))
    column(0)
    take("down", wdn, column_of(2))
    take_x("down", wdn, column_of(1))
    column(1)
    take("down", wdn, column_of(3))
    owned(0)
    take_x("down", wdn, column_of(2))
    column(2)
    owned(1)
    take_x("down", wdn, column_of(3))
    column(3)
    owned(2)
    owned(3)
    for s in range(fs - 1):
        sent.append(("sum_z", token_of(s), send_z.at[0], None))
    arrive("sum_y", fs - 1, got_y.at[i])
    branch = mine[i] + got_y[i].astype(f32)
    for s in range(fs - 2, -1, -1):
        b = token_of(s)
        arrive("sum_z", b, got_z.at[b])
        branch += got_z[b].astype(f32)
    held[...] = (rows[j, i].astype(f32) + branch).astype(bf16)
    out_copy = pltpu.make_async_copy(held, result_ref, local_sem.at[0])
    out_copy.start()
    for name, sk, block, given in sent:
        def done():
            copy(name, block, block, core, sk, sk).wait_send()

        if given is None:
            done()
        else:
            pl.when(given)(done)
    out_copy.wait()


def kernel_body(fs, tp, stream, mixed, out_weight, norm_gain, up_weight, down_weight):
    tokens, width = stream.shape
    half = out_weight.shape[0] // 2
    slots, count = slot_table(fs)
    vmem, anywhere = pl.BlockSpec(memory_space=pltpu.VMEM), pl.BlockSpec(memory_space=pl.ANY)
    weights = pltpu.VMEM((fs, 2, half, width), jnp.bfloat16)
    blocks = pltpu.VMEM((fs, tokens, width), jnp.bfloat16)
    columns = pltpu.VMEM((2, fs, tokens, width), jnp.bfloat16)
    sums = pltpu.VMEM((fs, tokens, width), jnp.float32)
    return pl.pallas_call(
        functools.partial(layer_kernel, fs, slots),
        out_shape=jax.ShapeDtypeStruct((tokens, width), jnp.bfloat16),
        in_specs=[anywhere, anywhere, anywhere, vmem, anywhere, anywhere],
        out_specs=anywhere,
        scratch_shapes=[
            pltpu.VMEM((tp, tokens, width), jnp.bfloat16),
            pltpu.VMEM((tp, 1, width), jnp.bfloat16),
            weights, weights, weights,
            pltpu.VMEM((tp, fs, tokens, width), jnp.bfloat16),
            blocks,
            sums, sums,
            columns, columns, blocks, blocks, blocks, blocks,
            pltpu.VMEM((tokens, width), jnp.bfloat16),
            pltpu.SemaphoreType.DMA((count,)),
            pltpu.SemaphoreType.DMA((count,)),
            pltpu.SemaphoreType.DMA((8,)),
        ],
        compiler_params=pltpu.CompilerParams(
            collective_id=0, has_side_effects=True, vmem_limit_bytes=56 * 1024 * 1024
        ),
    )(stream, mixed, out_weight, norm_gain, up_weight, down_weight)


def solution(mesh):
    placed = (
        P(("grp", "fs"), "tp"),
        P(("grp", "fs"), "tp"),
        P("fs", "tp"),
        P("tp"),
        P("fs", "tp"),
        P("tp", "fs"),
    )
    fs, tp = mesh.shape["fs"], mesh.shape["tp"]

    def call(stream, mixed, out_weight, norm_gain, up_weight, down_weight):
        width, hidden = up_weight.shape
        tokens = stream.shape[0] // mesh.shape["grp"]
        moved_weights = 2 * width * hidden // tp
        moved_rows = 2 * tokens * width + 2 * width * hidden // (tp * fs)
        aligned = fs == tp == 4 and (width // tp) % 256 == 0 and (tokens // fs) % 16 == 0
        aligned = aligned and hidden == tp * width
        body = spread_body if moved_rows < moved_weights else gathered_body
        if aligned and moved_rows < moved_weights:
            body = functools.partial(kernel_body, fs, tp)
        return sharded(body)(stream, mixed, out_weight, norm_gain, up_weight, down_weight)

    def sharded(body):
        return jax.shard_map(
            body, mesh=mesh, in_specs=placed, out_specs=P(("grp", "fs"), "tp"), check_vma=False
        )

    return call
```

time: 124 us -> 116 us (0.935)
  the two profiles are of different devices: /device:TPU:1 before, /device:TPU:8 now
where the time goes in v1:
time: 116 us; the launch traced here: 114 us
  Pallas kernels  112 us (97%)
  local copies, waits for them, and re-layouts  1.67 us (1%)
    pallas_call x1, Pallas kernels, kernel_body(): pl.pallas_call(functools.partial(layer_kernel, fs, slots), out_shape=jax....  112 us

profile of v1, /device:TPU:8, one launch (start us, length us, event | category | flops | bytes accessed | tf_op | source)
XLA Modules:
  0.0 113.6 jit_solution(6782695257459711868)
XLA Ops:
  0.0 111.9 %shard_map.64 = bf16[256,512]{1,0:T(8,128)(2,1)} custom-call(bf16[256,512]{1,0:T(8,128)(2,1)} %stream_ref.1, bf16[256,512]{1,0:T(8,128)(2,1)} %mixed_ref.1, bf16[512,512]{1,0:T(8,128)(2,1)} %out_ref.1, bf16[512]{0:T(512)(128)(2,1)} %gain_ref.1, bf16[512,2048]{1,0:T(8,128)(2,1)} %up_ref.1, bf16[2048,512]{1,0:T(8,128)(2,1)} %down_ref.1), custom_call_target="tpu_custom_call" | custom-call | tf_op jit(solution)/shard_map/pallas_call | solution.py:473
  111.9 1.7 %copy.8 = bf16[256,512]{1,0:T(8,128)(2,1)} copy(bf16[256,512]{1,0:T(8,128)(2,1)} %shard_map.64) | data formatting | bytes 524288

commit v2 on v0

v2 whole, which is shorter than its diff:
```python
import functools

import jax
import jax.numpy as jnp
from jax import lax
from jax.experimental import pallas as pl
from jax.experimental.pallas import tpu as pltpu
from jax.sharding import PartitionSpec as P

epsilon = 1e-06


def fold_product(left, portion):
    return jnp.dot(left, portion, preferred_element_type=jnp.float32)


def gathered_body(stream, mixed, out_weight, norm_gain, up_weight, down_weight):
    mixed_whole = lax.all_gather(mixed, "tp", axis=1, tiled=True)
    projected = fold_product(mixed_whole, lax.all_gather(out_weight, "fs", axis=0, tiled=True))
    resid = (stream.astype(jnp.float32) + projected).astype(jnp.bfloat16)
    widened = resid.astype(jnp.float32)
    resid_whole, gain_whole = (
        lax.all_gather(resid, "tp", axis=1, tiled=True),
        lax.all_gather(norm_gain, "tp", axis=0, tiled=True),
    )
    stream_wide = resid_whole.astype(jnp.float32)
    energy = jnp.mean(stream_wide * stream_wide, axis=1, keepdims=True)
    normed_whole = (
        stream_wide * lax.rsqrt(energy + epsilon) * gain_whole.astype(jnp.float32)
    ).astype(jnp.bfloat16)
    up_full = lax.all_gather(up_weight, "fs", axis=0, tiled=True)
    up_values = jnp.dot(normed_whole, up_full, preferred_element_type=jnp.float32)
    activated = jnp.square(jax.nn.relu(up_values)).astype(jnp.bfloat16)
    partials = jnp.dot(
        activated,
        lax.all_gather(down_weight, "fs", axis=1, tiled=True),
        preferred_element_type=jnp.float32,
    )
    branch = lax.psum_scatter(partials, "tp", scatter_dimension=1, tiled=True)
    return (widened + branch).astype(jnp.bfloat16)


def spread_body(stream, mixed, out_weight, norm_gain, up_weight, down_weight):
    mixed_whole = lax.all_gather(mixed, "tp", axis=1, tiled=True)
    out_full = lax.all_gather(out_weight, "fs", axis=0, tiled=True)
    up_mine = lax.all_to_all(up_weight, "fs", split_axis=1, concat_axis=0, tiled=True)
    down_mine = lax.all_to_all(down_weight, "fs", split_axis=0, concat_axis=1, tiled=True)
    projected = jnp.dot(mixed_whole, out_full, preferred_element_type=jnp.float32)
    resid = (stream.astype(jnp.float32) + projected).astype(jnp.bfloat16)
    rows = lax.all_gather(resid, "fs", axis=0, tiled=True)
    whole = lax.all_gather(rows, "tp", axis=1, tiled=True).astype(jnp.float32)
    gain = lax.all_gather(norm_gain, "tp", axis=0, tiled=True).astype(jnp.float32)
    energy = jnp.mean(whole * whole, axis=1, keepdims=True)
    normed = (whole * lax.rsqrt(energy + epsilon) * gain).astype(jnp.bfloat16)
    up_values = jnp.dot(normed, up_mine, preferred_element_type=jnp.float32)
    activated = jnp.square(jax.nn.relu(up_values)).astype(jnp.bfloat16)
    partials = jnp.dot(activated, down_mine, preferred_element_type=jnp.float32).astype(jnp.bfloat16)
    columns = lax.psum_scatter(partials, "tp", scatter_dimension=1, tiled=True)
    branch = lax.psum_scatter(columns, "fs", scatter_dimension=0, tiled=True)
    return (resid.astype(jnp.float32) + branch.astype(jnp.float32)).astype(jnp.bfloat16)


MESH = pl.DeviceIdType.MESH


PARTS = dict(out=2, up=2, down=2, rows=2)

SCRIPTS = {
    (0, 0): [
        10, 11, 900, 210, 310, 211, 1000, 311, 120, 320, 131, 321, 430, 121, 130, 610, 110, 530, 330, 111,
        331, 431, 1100, 620, 630, 1800, 1310, 1400, 1311, 531, 1600, 1410, 410, 411, 1510, 1610, 420, 1511,
        1611, 1520, 230, 1601, 421, 231, 220, 221, 1620, 1621, 1521, 1530, 1200, 710, 720, 730, 1700, 1900,
        1710, 1910, 1720, 1920, 1531, 1999, 2020, 830, 2023, 2010, 2013, 1630, 2123, 1999, 2000, 1999, 2120,
        2199, 2003, 2110, 520, 2199, 2099, 2099, 2199, 2099, 2100, 521, 1631, 1730, 2199, 1930, 2030, 2130,
        2033, 2133, 510, 820, 2032, 2022, 2012, 2113, 2103, 2199, 511, 2132, 2122, 2002, 2299, 2112, 2102,
        810, 2011, 2031, 2021, 2001, 2131, 2121, 2111, 2230, 2101, 2220, 2210, 2299, 2300,
    ],
    (0, 1): [
        900, 10, 11, 211, 210, 1000, 230, 130, 310, 321, 320, 311, 120, 330, 121, 620, 231, 331, 131, 430,
        110, 431, 1100, 610, 630, 1800, 1310, 1400, 1311, 421, 420, 1410, 1600, 111, 1510, 720, 410, 411,
        1601, 1511, 1610, 1520, 1200, 710, 730, 1700, 1900, 1999, 1999, 1999, 2000, 2099, 2099, 2099, 1521,
        1611, 1710, 2199, 1910, 1620, 2010, 530, 1530, 1621, 1720, 531, 1920, 2100, 2199, 2020, 1630, 1531,
        2120, 2110, 830, 2003, 2023, 2199, 2013, 2103, 221, 220, 510, 2113, 1631, 1730, 1930, 511, 2033, 2123,
        2030, 2130, 520, 810, 2031, 2001, 2021, 2199, 2133, 2199, 2131, 2101, 2011, 2299, 2121, 521, 2111,
        820, 2022, 2032, 2002, 2012, 2132, 2102, 2122, 2230, 2112, 2220, 2210, 2299, 2300,
    ],
    (1, 0): [
        20, 21, 0, 900, 1, 300, 320, 1000, 301, 321, 330, 500, 130, 331, 131, 501, 430, 100, 431, 101, 600,
        620, 630, 1100, 1800, 1300, 1400, 1301, 1320, 1321, 1410, 1610, 1611, 120, 1520, 400, 121, 401, 1521,
        1620, 1500, 420, 1621, 1501, 1600, 1530, 220, 1601, 1531, 1630, 1631, 221, 421, 520, 730, 1200, 1710,
        700, 720, 1910, 1700, 1900, 230, 521, 1720, 1920, 1730, 1930, 800, 820, 2030, 2031, 2010, 231, 200,
        201, 2020, 2110, 1999, 2011, 1999, 2130, 2199, 2032, 2199, 2111, 2012, 2021, 2120, 2000, 2121, 2131,
        1999, 2099, 2132, 2001, 2100, 2002, 2022, 2099, 2199, 2199, 2112, 2122, 2101, 2099, 2200, 2102, 531,
        530, 830, 2199, 2023, 2033, 2013, 2003, 2133, 2113, 2123, 2299, 2103, 2230, 2220, 2299, 2300,
    ],
    (1, 1): [
        20, 900, 0, 1, 21, 300, 320, 1000, 301, 321, 330, 331, 1100, 500, 501, 430, 100, 431, 600, 101, 620,
        630, 1800, 1320, 1400, 1301, 1321, 1410, 1610, 120, 1300, 1520, 400, 130, 1611, 1521, 1500, 420, 1620,
        1501, 421, 401, 1621, 1600, 1530, 131, 1601, 121, 1630, 730, 220, 1531, 1200, 700, 720, 1710, 1910,
        1700, 1900, 1720, 1920, 1631, 1999, 2001, 800, 221, 2000, 2021, 1730, 2099, 2100, 1930, 2099, 230,
        1999, 2199, 2121, 200, 2031, 2199, 2101, 2020, 2030, 2199, 2011, 2131, 2199, 1999, 2010, 2130, 2099,
        2111, 201, 231, 530, 531, 520, 521, 830, 2003, 2023, 2033, 2120, 2199, 2110, 2103, 2123, 2013, 2299,
        2133, 2113, 820, 2032, 2002, 2022, 2012, 2102, 2122, 2132, 2299, 2112, 2230, 2200, 2220, 2300,
    ],
}


GROUPS = dict(z=0, x=1, mixed=1, y=2, c=2, d=2, sum_c=3, sum_y=4, sum_a=5, sum_z=5, gain=6)


def slot_table(fs):
    table, count = {}, 0
    sizes = dict(mixed=3, gain=1, sum_c=2 * fs, sum_y=fs, sum_a=2, sum_z=2, rows_c=fs, rows_d=fs)
    for name, parts in PARTS.items():
        sizes[name + "_z"] = fs * parts
        if name == "rows":
            sizes["rows_y"] = fs * parts
        else:
            sizes[name + "_x"] = fs
    for name, size in sizes.items():
        table[name] = count
        count += size
    return table, count


LETTERS, TWO, ONE = "AUDaudxvzmnlgBybrwPHCFOE", "AUDaudBbrCF", "xvzywHO"


def unpack(code):
    kind, rest = LETTERS[code // 100], code % 100
    if rest == 99:
        return kind, None
    count = 2 if kind in TWO else 1 if kind in ONE else 0
    return kind, [rest // 10, rest % 10][:count]


def segments(script):
    parts, steps = [[]], []
    for token in map(unpack, script):
        if token[0] in "PHCFOE":
            steps.append(token)
            parts.append([])
        else:
            parts[-1].append(token)
    return parts, steps


def layer_kernel(
    fs, slots,
    stream_ref, mixed_ref, out_ref, gain_ref, up_ref, down_ref, result_ref,
    mixw, gains, wo, wup, wdn, rows, acts, kept, send_c, got_c, send_y, got_y, send_z, got_a, got_z,
    held, send_sem, recv_sem, local_sem,
):
    f32, bf16 = jnp.float32, jnp.bfloat16
    g, i, j = lax.axis_index("grp"), lax.axis_index("fs"), lax.axis_index("tp")
    y, c = j // 2, j % 2
    jc = y * 2 + (1 - c)
    jy = (1 - y) * 2 + c
    jd = (1 - y) * 2 + (1 - c)
    half, width = wo.shape[2], wo.shape[3]

    low = i < fs // 2
    v = jnp.where(low, i, fs - 1 - i)
    yr = jnp.where(low, y, 1 - y)
    cr = jnp.where(low, c, 1 - c)

    def real(w):
        return jnp.where(low, w, fs - 1 - w)

    core, across, diag, twin = (g, i, jc), (g, i, jy), (g, i, jd), (1 - g, i, j)
    both = jnp.logical_and

    def at(w):
        return (g, real(w), j)

    def group(name):
        return GROUPS[name] if name in GROUPS else GROUPS[name.split("_")[1]]

    def copy(name, src, dst, target, rk):
        return pltpu.make_async_remote_copy(
            src_ref=src, dst_ref=dst,
            send_sem=send_sem.at[group(name)], recv_sem=recv_sem.at[slots[name] + rk],
            device_id=target, device_id_type=MESH,
        )

    def send(name, src, dst, target, rk):
        copy(name, src, dst, target, rk).start()

    def arrive(name, rk, dst):
        copy(name, dst, dst, core, rk).wait_recv()

    barrier = pltpu.get_barrier_semaphore()
    greeted = [core, across, diag, twin]
    for device in greeted:
        pl.semaphore_signal(barrier, inc=1, device_id=device, device_id_type=MESH)
    for s in range(1, fs):
        pl.semaphore_signal(barrier, inc=1, device_id=(g, lax.rem(i + s, fs), j), device_id_type=MESH)

    def keep(src, dst):
        pltpu.make_async_copy(src, dst, local_sem.at[0]).start()

    def up_piece(owner, part):
        return up_ref.at[pl.ds(part * half, half), pl.ds(pl.multiple_of(owner * width, width), width)]

    def down_piece(owner, part):
        return down_ref.at[pl.ds(owner * 2 * half + part * half, half), :]

    for part in range(2):
        keep(out_ref.at[pl.ds(part * half, half), :], wo.at[i, part])
        keep(up_piece(i, part), wup.at[i, part])
        keep(down_piece(i, part), wdn.at[i, part])
    keep(mixed_ref, mixw.at[j])
    keep(stream_ref, held)
    gains[j] = gain_ref[...].astype(f32).reshape(1, width).astype(bf16)
    pl.semaphore_wait(barrier, len(greeted) + fs - 1)

    def piece(name, ref, q):
        size = ref.shape[0] // PARTS[name]
        return ref.at[pl.ds(q * size, size), :]

    def block_of(name, w):
        if name == "rows":
            return rows.at[j, real(w)]
        return dict(out=wo, up=wup, down=wdn)[name].at[real(w), g]

    def slot(name, b, q):
        return real(b) * PARTS[name] + q

    def pass_on(name, b, q, to):
        block = piece(name, block_of(name, b), q)
        send(name + "_z", block, block, at(to), slot(name, b, q))

    def crossing(b, q):
        block = piece("rows", block_of("rows", b), q)
        send("rows_y", block, block, across, slot("rows", b, q))
        send("rows_c", block, block, core, real(b))

    def twin_copy(name, b, q):
        block = piece(name, block_of(name, b), q)
        send(name + "_x", block, block, twin, real(b))

    def act(own, token):
        kind, args = token
        if kind in "AUD":
            w, q = args
            name = dict(A="out", U="up", D="down")[kind]
            to = real(w)
            source = dict(
                A=out_ref.at[pl.ds(g * half, half), :], U=up_piece(to, g), D=down_piece(to, g)
            )[kind]
            send(
                name + "_z", piece(name, source, q), piece(name, block_of(name, own), q), at(w),
                slot(name, own, q),
            )
        elif kind in "aud":
            b, q = args
            name = dict(a="out", u="up", d="down")[kind]
            arrive(name + "_z", slot(name, b, q), piece(name, block_of(name, b), q))
            if kind == "a":
                to = own + 1 if b < own else own - 1
                if to >= 0:
                    pass_on(name, b, q, to)
            twin_copy(name, b, q)
        elif kind in "xvz":
            (b,) = args
            name, buffer = dict(x=("out", wo), v=("up", wup), z=("down", wdn))[kind]
            arrive(name + "_x", real(b), buffer.at[real(b), 1 - g])
        elif kind == "m":
            send("mixed", mixed_ref, mixw.at[j], across, 0)
            send("mixed", mixed_ref, mixw.at[j], core, 1)
            for target in (across, core, diag):
                send("gain", gains.at[j], gains.at[j], target, 0)
        elif kind == "n":
            arrive("mixed", 0, mixw.at[jy])
            send("mixed", mixw.at[jy], mixw.at[jy], core, 2)
        elif kind == "l":
            arrive("mixed", 1, mixw.at[jc])
            arrive("mixed", 2, mixw.at[jd])
        elif kind == "g":
            arrive("gain", 0, gains.at[pl.ds(0, 3)])
        elif kind == "B":
            w, q = args
            pass_on("rows", own, q, w)
        elif kind == "y":
            (q,) = args
            crossing(own, q)
        elif kind == "b":
            b, q = args
            arrive("rows_z", slot("rows", b, q), piece("rows", block_of("rows", b), q))
            to = own + 1 if b < own else own - 1
            if to >= 0:
                pass_on("rows", b, q, to)
            crossing(b, q)
        elif kind == "r":
            b, q = args
            block = piece("rows", rows.at[jy, real(b)], q)
            arrive("rows_y", slot("rows", b, q), block)
            send("rows_d", block, block, core, real(b))
        elif kind == "w":
            (b,) = args
            arrive("rows_c", real(b), rows.at[jc, real(b)])
            arrive("rows_d", real(b), rows.at[jd, real(b)])

    def whole(ref, k):
        return ref[k].reshape(2 * half, width)

    kinds = [(a, b) for a in range(2) for b in range(2)]
    plans = [segments(SCRIPTS[kind]) for kind in kinds]

    def pick(values):
        lower = values[0] if values[0] == values[1] else jnp.where(yr == 0, values[0], values[1])
        upper = values[2] if values[2] == values[3] else jnp.where(yr == 0, values[2], values[3])
        if list(values[:2]) == list(values[2:]):
            return lower
        return jnp.where(v == 0, lower, upper)

    def project():
        pltpu.make_async_copy(send_c, got_c, local_sem.at[0]).wait()
        total = held[...].astype(f32)
        for k in range(fs):
            total += jnp.dot(mixw[k], whole(wo, k), preferred_element_type=f32)
        rows[j, i] = total.astype(bf16)

    def hidden(t):
        z = real(t)
        wide = [rows[k, z].astype(f32) for k in range(rows.shape[0])]
        energy = sum(jnp.sum(w * w, axis=1, keepdims=True) for w in wide)
        scale = lax.rsqrt(energy * (1.0 / (len(wide) * width)) + epsilon)
        up = None
        for k, w in enumerate(wide):
            normed = (w * scale * gains[k].astype(f32)).astype(bf16)
            term = jnp.dot(normed, whole(wup, k), preferred_element_type=f32)
            up = term if up is None else up + term
        acts[t] = jnp.square(jnp.maximum(up, 0.0)).astype(bf16)

    def column(t, k):
        p = k // 2
        part = jnp.dot(acts[t], whole(wdn, real(k)), preferred_element_type=f32)

        @pl.when(k % 2 != cr)
        def _():
            send_c[p, t] = part.astype(bf16)
            copy("sum_c", send_c.at[p, t], got_c.at[p, t], core, p * fs + t).start()

        @pl.when(k % 2 == cr)
        def _():
            kept[p, t] = part

    def fold(t, k):
        p = k // 2

        @pl.when(k % 2 == cr)
        def _():
            arrive("sum_c", p * fs + t, got_c.at[p, t])
            kept[p, t] = kept[p, t] + got_c[p, t].astype(f32)

            @pl.when(p != yr)
            def _():
                send_y[t] = kept[p, t].astype(bf16)
                copy("sum_y", send_y.at[t], got_y.at[t], across, t).start()

    def offer(t):
        arrive("sum_y", t, got_y.at[t])
        joined = both(v == 1, t >= fs // 2)
        first = both(v == 0, t >= fs // 2)
        kept[yr, t] = kept[yr, t] + got_y[t].astype(f32)

        @pl.when(joined)
        def _():
            arrive("sum_a", t - fs // 2, got_a.at[t - fs // 2])
            send_z[t] = (kept[yr, t] + got_a[t - fs // 2].astype(f32)).astype(bf16)
            copy("sum_z", send_z.at[t], got_z.at[1], at(t), 1).start()

        @pl.when(first)
        def _():
            send_z[t] = kept[yr, t].astype(bf16)
            copy("sum_a", send_z.at[t], got_a.at[t - fs // 2], at(1), t - fs // 2).start()

        @pl.when(t < fs // 2)
        def _():
            send_z[t] = kept[yr, t].astype(bf16)
            copy("sum_z", send_z.at[t], got_z.at[0], at(t), 0).start()

    def finish():
        arrive("sum_y", v, got_y.at[v])
        branch = kept[yr, v] + got_y[v].astype(f32)
        for n in range(2):
            arrive("sum_z", n, got_z.at[n])
            branch += got_z[n].astype(f32)
        held[...] = (rows[j, i].astype(f32) + branch).astype(bf16)

    mine = [v == own for own in range(2)]
    exact = [[both(mine[own], yr == b) for b in range(2)] for own in range(2)]
    for n in range(len(plans[0][0])):
        for own in range(2):
            lists = [plans[2 * own + b][0][n] for b in range(2)]
            if lists[0] == lists[1]:
                if lists[0]:
                    @pl.when(mine[own])
                    def _():
                        for token in lists[0]:
                            act(own, token)
            else:
                for b in range(2):
                    if lists[b]:
                        given = exact[own][b]

                        @pl.when(given)
                        def _():
                            for token in lists[b]:
                                act(own, token)
        if n < len(plans[0][1]):
            steps = [plan[1][n] for plan in plans]
            kind = steps[0][0]
            taken = [step[1] is not None for step in steps]
            if not any(taken):
                continue
            default = steps[taken.index(True)]
            choices = [step[1] if used else default[1] for step, used in zip(steps, taken)]
            args = [pick(list(values)) for values in zip(*choices)]
            run = dict(P=project, H=hidden, C=column, F=fold, O=offer, E=finish)[kind]
            if all(taken):
                run(*args)
            else:
                here = functools.reduce(
                    jnp.logical_or, [one for one, used in zip(exact[0] + exact[1], taken) if used]
                )
                pl.when(here)(functools.partial(run, *args))

    out_copy = pltpu.make_async_copy(held, result_ref, local_sem.at[1])
    out_copy.start()

    def drain(name, total):
        copy(name, total, total, core, 0).wait_send()

    @pl.when(v == 0)
    def _():
        drain("out_z", got_c)

    @pl.when(v == 1)
    def _():
        drain("out_z", rows)

    drain("mixed", rows.at[pl.ds(0, 3)])
    drain("rows_y", rows.at[pl.ds(0, 3)])
    drain("sum_c", got_c)
    drain("sum_y", got_y)
    drain("sum_z", send_z.at[pl.ds(0, 3)])
    drain("gain", gains.at[pl.ds(0, 3)])
    out_copy.wait()


def kernel_body(fs, tp, stream, mixed, out_weight, norm_gain, up_weight, down_weight):
    tokens, width = stream.shape
    half = out_weight.shape[0] // 2
    slots, count = slot_table(fs)
    vmem, anywhere = pl.BlockSpec(memory_space=pltpu.VMEM), pl.BlockSpec(memory_space=pl.ANY)
    weights = pltpu.VMEM((fs, 2, half, width), jnp.bfloat16)
    blocks = pltpu.VMEM((fs, tokens, width), jnp.bfloat16)
    columns = pltpu.VMEM((2, fs, tokens, width), jnp.bfloat16)
    pair = pltpu.VMEM((2, tokens, width), jnp.bfloat16)
    return pl.pallas_call(
        functools.partial(layer_kernel, fs, slots),
        out_shape=jax.ShapeDtypeStruct((tokens, width), jnp.bfloat16),
        in_specs=[anywhere, anywhere, anywhere, vmem, anywhere, anywhere],
        out_specs=anywhere,
        scratch_shapes=[
            pltpu.VMEM((tp, tokens, width), jnp.bfloat16),
            pltpu.VMEM((tp, 1, width), jnp.bfloat16),
            weights, weights, weights,
            pltpu.VMEM((tp, fs, tokens, width), jnp.bfloat16),
            blocks,
            pltpu.VMEM((2, fs, tokens, width), jnp.float32),
            columns, columns, blocks, blocks, blocks, pair, pair,
            pltpu.VMEM((tokens, width), jnp.bfloat16),
            pltpu.SemaphoreType.DMA((7,)),
            pltpu.SemaphoreType.DMA((count,)),
            pltpu.SemaphoreType.DMA((2,)),
        ],
        compiler_params=pltpu.CompilerParams(
            collective_id=0, has_side_effects=True, vmem_limit_bytes=56 * 1024 * 1024
        ),
    )(stream, mixed, out_weight, norm_gain, up_weight, down_weight)


def solution(mesh):
    placed = (
        P(("grp", "fs"), "tp"),
        P(("grp", "fs"), "tp"),
        P("fs", "tp"),
        P("tp"),
        P("fs", "tp"),
        P("tp", "fs"),
    )
    fs, tp = mesh.shape["fs"], mesh.shape["tp"]

    def call(stream, mixed, out_weight, norm_gain, up_weight, down_weight):
        width, hidden = up_weight.shape
        tokens = stream.shape[0] // mesh.shape["grp"]
        moved_weights = 2 * width * hidden // tp
        moved_rows = 2 * tokens * width + 2 * width * hidden // (tp * fs)
        aligned = fs == tp == 4 and (width // tp) % 256 == 0 and (tokens // fs) % 16 == 0
        aligned = aligned and hidden == tp * width
        body = spread_body if moved_rows < moved_weights else gathered_body
        if aligned and moved_rows < moved_weights:
            body = functools.partial(kernel_body, fs, tp)
        return sharded(body)(stream, mixed, out_weight, norm_gain, up_weight, down_weight)

    def sharded(body):
        return jax.shard_map(
            body, mesh=mesh, in_specs=placed, out_specs=P(("grp", "fs"), "tp"), check_vma=False
        )

    return call
```

time: 124 us -> 111 us (0.90)
  the two profiles are of different devices: /device:TPU:1 before, /device:TPU:8 now
where the time goes in v2:
time: 111 us
  Pallas kernels  109 us (98%)
  local copies, waits for them, and re-layouts  1.67 us (2%)
    pallas_call x1, Pallas kernels, kernel_body(): pl.pallas_call(functools.partial(layer_kernel, fs, slots), out_shape=jax....  109 us

profile of v2, /device:TPU:8, one launch (start us, length us, event | category | flops | bytes accessed | tf_op | source)
XLA Modules:
  0.0 110.8 jit_solution(10455727619987651600)
XLA Ops:
  0.0 109.2 %shard_map.64 = bf16[256,512]{1,0:T(8,128)(2,1)} custom-call(bf16[256,512]{1,0:T(8,128)(2,1)} %stream_ref.1, bf16[256,512]{1,0:T(8,128)(2,1)} %mixed_ref.1, bf16[512,512]{1,0:T(8,128)(2,1)} %out_ref.1, bf16[512]{0:T(512)(128)(2,1)} %gain_ref.1, bf16[512,2048]{1,0:T(8,128)(2,1)} %up_ref.1, bf16[2048,512]{1,0:T(8,128)(2,1)} %down_ref.1), custom_call_target="tpu_custom_call" | custom-call | tf_op jit(solution)/shard_map/pallas_call | solution.py:462
  109.2 1.7 %copy.8 = bf16[256,512]{1,0:T(8,128)(2,1)} copy(bf16[256,512]{1,0:T(8,128)(2,1)} %shard_map.64) | data formatting | bytes 524288

commit v3 on v2

--- a/solution.py
+++ b/solution.py
@@ -110,7 +110,7 @@
 
 def slot_table(fs):
     table, count = {}, 0
-    sizes = dict(mixed=3, gain=1, sum_c=2 * fs, sum_y=fs, sum_a=2, sum_z=2, rows_c=fs, rows_d=fs)
+    sizes = dict(mixed=3, gain=1, sum_c=2 * fs, sum_y=2 * fs, sum_a=4, sum_z=4, rows_c=fs, rows_d=fs)
     for name, parts in PARTS.items():
         sizes[name + "_z"] = fs * parts
         if name == "rows":
@@ -346,48 +346,56 @@
         def _():
             kept[p, t] = part
 
+    tokens = held.shape[0]
+    spans = [pl.ds(h * (tokens // 2), tokens // 2) for h in range(2)]
+
     def fold(t, k):
         p = k // 2
 
         @pl.when(k % 2 == cr)
         def _():
             arrive("sum_c", p * fs + t, got_c.at[p, t])
-            kept[p, t] = kept[p, t] + got_c[p, t].astype(f32)
 
             @pl.when(p != yr)
             def _():
-                send_y[t] = kept[p, t].astype(bf16)
-                copy("sum_y", send_y.at[t], got_y.at[t], across, t).start()
+                for h, span in enumerate(spans):
+                    send_y[t, span] = (kept[p, t, span] + got_c[p, t, span].astype(f32)).astype(bf16)
+                    copy("sum_y", send_y.at[t, span], got_y.at[t, span], across, 2 * t + h).start()
+
+            @pl.when(p == yr)
+            def _():
+                kept[p, t] = kept[p, t] + got_c[p, t].astype(f32)
 
     def offer(t):
-        arrive("sum_y", t, got_y.at[t])
-        joined = both(v == 1, t >= fs // 2)
-        first = both(v == 0, t >= fs // 2)
-        kept[yr, t] = kept[yr, t] + got_y[t].astype(f32)
-
-        @pl.when(joined)
-        def _():
-            arrive("sum_a", t - fs // 2, got_a.at[t - fs // 2])
-            send_z[t] = (kept[yr, t] + got_a[t - fs // 2].astype(f32)).astype(bf16)
-            copy("sum_z", send_z.at[t], got_z.at[1], at(t), 1).start()
-
-        @pl.when(first)
-        def _():
-            send_z[t] = kept[yr, t].astype(bf16)
-            copy("sum_a", send_z.at[t], got_a.at[t - fs // 2], at(1), t - fs // 2).start()
-
-        @pl.when(t < fs // 2)
-        def _():
-            send_z[t] = kept[yr, t].astype(bf16)
-            copy("sum_z", send_z.at[t], got_z.at[0], at(t), 0).start()
+        e = t - fs // 2
+        for h, span in enumerate(spans):
+            arrive("sum_y", 2 * t + h, got_y.at[t, span])
+
+            @pl.when(both(v == 1, t >= fs // 2))
+            def _():
+                arrive("sum_a", 2 * e + h, got_a.at[e, span])
+                part = kept[yr, t, span] + got_y[t, span].astype(f32) + got_a[e, span].astype(f32)
+                send_z[t, span] = part.astype(bf16)
+                copy("sum_z", send_z.at[t, span], got_z.at[1, span], at(t), 2 + h).start()
+
+            @pl.when(both(v == 0, t >= fs // 2))
+            def _():
+                send_z[t, span] = (kept[yr, t, span] + got_y[t, span].astype(f32)).astype(bf16)
+                copy("sum_a", send_z.at[t, span], got_a.at[e, span], at(1), 2 * e + h).start()
+
+            @pl.when(t < fs // 2)
+            def _():
+                send_z[t, span] = (kept[yr, t, span] + got_y[t, span].astype(f32)).astype(bf16)
+                copy("sum_z", send_z.at[t, span], got_z.at[0, span], at(t), h).start()
 
     def finish():
-        arrive("sum_y", v, got_y.at[v])
-        branch = kept[yr, v] + got_y[v].astype(f32)
-        for n in range(2):
-            arrive("sum_z", n, got_z.at[n])
-            branch += got_z[n].astype(f32)
-        held[...] = (rows[j, i].astype(f32) + branch).astype(bf16)
+        for h, span in enumerate(spans):
+            arrive("sum_y", 2 * v + h, got_y.at[v, span])
+            branch = kept[yr, v, span] + got_y[v, span].astype(f32)
+            for n in range(2):
+                arrive("sum_z", 2 * n + h, got_z.at[n, span])
+                branch += got_z[n, span].astype(f32)
+            held[span] = (rows[j, i, span].astype(f32) + branch).astype(bf16)
 
     mine = [v == own for own in range(2)]
     exact = [[both(mine[own], yr == b) for b in range(2)] for own in range(2)]

time: 111 us -> 109 us (0.982)
  Pallas kernels: 109 us -> 107 us
    pallas_call x1, Pallas kernels: 109 us -> 107 us  [kernel_body(): pl.pallas_call(functools.partial(layer_kernel, fs, slots), out_shape=jax....]
where the time goes in v3:
time: 109 us
  Pallas kernels  107 us (98%)
  local copies, waits for them, and re-layouts  1.67 us (2%)
    pallas_call x1, Pallas kernels, kernel_body(): pl.pallas_call(functools.partial(layer_kernel, fs, slots), out_shape=jax....  107 us

profile of v3, /device:TPU:8, one launch (start us, length us, event | category | flops | bytes accessed | tf_op | source)
XLA Modules:
  0.0 108.8 jit_solution(4356129715101862548)
XLA Ops:
  0.0 107.1 %shard_map.64 = bf16[256,512]{1,0:T(8,128)(2,1)} custom-call(bf16[256,512]{1,0:T(8,128)(2,1)} %stream_ref.1, bf16[256,512]{1,0:T(8,128)(2,1)} %mixed_ref.1, bf16[512,512]{1,0:T(8,128)(2,1)} %out_ref.1, bf16[512]{0:T(512)(128)(2,1)} %gain_ref.1, bf16[512,2048]{1,0:T(8,128)(2,1)} %up_ref.1, bf16[2048,512]{1,0:T(8,128)(2,1)} %down_ref.1), custom_call_target="tpu_custom_call" | custom-call | tf_op jit(solution)/shard_map/pallas_call | solution.py:470
  107.2 1.7 %copy.8 = bf16[256,512]{1,0:T(8,128)(2,1)} copy(bf16[256,512]{1,0:T(8,128)(2,1)} %shard_map.64) | data formatting | bytes 524288
